TPU v7x, 32 devices: a whole 2x2x4 slice. The times are simulated.
32 devices in a mesh: sp: 8 (over z, y), tp: 4 (over x, core).
Axes of the slice: x: 2, y: 2, z: 4, core: 2. Of those that a mesh axis runs over, the one named last changes fastest.
Arguments:
- inputs: bfloat16 [8192, 2048], P('sp'), may hold values from -6 to 6
- norm_gain: float32 [3, 2048], replicated, may hold values from 0.1 to 1.9
- query_weight: bfloat16 [3, 2048, 1024], P(None, 'sp', 'tp'), may hold values from -64 to 64
- key_weight: bfloat16 [3, 2048, 512], P(None, 'sp', 'tp'), may hold values from -4 to 4
- value_weight: bfloat16 [3, 2048, 512], P(None, 'sp', 'tp'), may hold values from -0.125 to 0.125
- output_weight: bfloat16 [3, 2048, 1024], P(None, 'sp', 'tp'), may hold values from -0.1875 to 0.1875
- sink_logit: float32 [3, 16], P(None, 'tp'), may hold values from 2 to 7
- final_gain: float32 [2048], replicated, may hold values from 0.1 to 1.9
Outputs:
- result: float32 [8192, 2048], P(('sp', 'tp'))
All inputs are finite; a program needn't handle non-finite values.
Results may differ from a plain program's by a relative error of at most 0.015.
Values may be sent and summed in bfloat16 or wider, within the bound.
A program may use at most 64 MiB of HBM per device.

v0:
```python
import jax
import jax.numpy as jnp
from jax import lax
from jax.sharding import PartitionSpec as P

D = 2048
HEAD_DIM = 64
WINDOW = 128
LAYERS = 3
EPS = 1e-06


def extended_2(block, sides, width):
    for axis, dim in sides:
        count = lax.axis_size(axis)
        forward = [(i, i + 1) for i in range(count - 1)]
        backward = [(target, source) for source, target in forward]
        low = lax.ppermute(
            lax.slice_in_dim(block, block.shape[dim] - width, None, axis=dim), axis, forward
        )
        high = lax.ppermute(lax.slice_in_dim(block, 0, width, axis=dim), axis, backward)
        block = jnp.concatenate([low, block, high], axis=dim)
    return block


def norm_rows(values, gain):
    wide_values = values.astype(jnp.float32)
    inv_root = lax.rsqrt(jnp.mean(wide_values * wide_values, axis=-1, keepdims=True) + EPS)
    return wide_values * inv_root * gain


def rotate(values, places):
    half_dim = values.shape[-1] // 2
    inverse = 10000.0 ** (-jnp.arange(half_dim).astype(jnp.float32) / half_dim)
    angles = places[:, None] * inverse[None, :]
    cosine_table = jnp.cos(angles)[:, None, :]
    sine_table = jnp.sin(angles)[:, None, :]
    front_half = values[..., :half_dim]
    back_half = values[..., half_dim:]
    return jnp.concatenate(
        [
            front_half * cosine_table - back_half * sine_table,
            back_half * cosine_table + front_half * sine_table,
        ],
        axis=-1,
    )


def attend(queries, key_rows, value_rows, sink_row, allowed):
    scores = jnp.einsum(
        "qkgd,skd->kgqs", queries, key_rows, preferred_element_type=jnp.float32
    ) * queries.shape[-1] ** (-0.5)
    scores = jnp.where(allowed[None, None], scores, -jnp.inf)
    sink_col = sink_row[:, :, None]
    largest = jnp.maximum(jnp.max(scores, axis=-1), sink_col)
    powers = jnp.exp(scores - largest[..., None])
    denominator = jnp.sum(powers, axis=-1) + jnp.exp(sink_col - largest)
    weights = (powers / denominator[..., None]).astype(jnp.bfloat16)
    blended = jnp.einsum("kgqs,skd->qkgd", weights, value_rows, preferred_element_type=jnp.float32)
    return blended.astype(jnp.bfloat16)


def shards(
    inputs, norm_gain, query_weight, key_weight, value_weight, output_weight, sink_logit, final_gain
):
    tokens = inputs.shape[0]
    local_heads = query_weight.shape[2] // HEAD_DIM
    local_groups = key_weight.shape[2] // HEAD_DIM
    per_group = local_heads // local_groups
    kv_cols = local_groups * HEAD_DIM
    offset = lax.axis_index("sp") * tokens
    seq_total = tokens * lax.axis_size("sp")
    query_pos = offset + jnp.arange(tokens, dtype=jnp.int32)
    places = query_pos.astype(jnp.float32)
    key_pos = offset - WINDOW + jnp.arange(tokens + 2 * WINDOW, dtype=jnp.int32)
    allowed = (
        (jnp.abs(key_pos[None, :] - query_pos[:, None]) <= WINDOW)
        & (key_pos[None, :] >= 0)
        & (key_pos[None, :] < seq_total)
    )
    whole_query, whole_key, whole_value, whole_out = (
        lax.all_gather(query_weight, "sp", axis=1, tiled=True),
        lax.all_gather(key_weight, "sp", axis=1, tiled=True),
        lax.all_gather(value_weight, "sp", axis=1, tiled=True),
        lax.all_gather(output_weight, "sp", axis=1, tiled=True),
    )
    current = inputs
    final_rows = inputs
    for layer in range(LAYERS):
        normed = norm_rows(current, norm_gain[layer]).astype(jnp.bfloat16)
        query_raw = jnp.dot(normed, whole_query[layer], preferred_element_type=jnp.float32)
        key_raw = jnp.dot(normed, whole_key[layer], preferred_element_type=jnp.float32)
        value_raw = jnp.dot(normed, whole_value[layer], preferred_element_type=jnp.float32)
        out_weight = whole_out[layer]
        queries = rotate(
            (query_raw * float(D) ** (-0.5)).reshape(tokens, local_heads, HEAD_DIM), places
        ).astype(jnp.bfloat16)
        key_rot = rotate(
            (key_raw * float(D) ** (-0.5)).reshape(tokens, local_groups, HEAD_DIM), places
        ).astype(jnp.bfloat16)
        packed = jnp.concatenate(
            [key_rot.reshape(tokens, kv_cols), value_raw.astype(jnp.bfloat16)], axis=1
        )
        extended = extended_2(packed, (("sp", 0),), WINDOW)
        key_rows = extended[:, :kv_cols].reshape(-1, local_groups, HEAD_DIM)
        value_all = extended[:, kv_cols:].reshape(-1, local_groups, HEAD_DIM)
        sink_row = sink_logit[layer].reshape(local_groups, per_group)
        attended = attend(
            queries.reshape(tokens, local_groups, per_group, HEAD_DIM),
            key_rows,
            value_all,
            sink_row,
            allowed,
        )
        attended = attended.reshape(tokens, local_heads * HEAD_DIM)

        def project():
            return lax.dot_general(
                attended, out_weight, (((1,), (1,)), ((), ())), preferred_element_type=jnp.float32
            )

        if layer < LAYERS - 1:
            share_rows = lax.psum_scatter(project(), "tp", scatter_dimension=0, tiled=True).astype(
                jnp.bfloat16
            )
            current = lax.all_gather(share_rows, "tp", axis=0, tiled=True)
        else:
            final_rows = lax.psum_scatter(
                project().astype(jnp.bfloat16), "tp", scatter_dimension=0, tiled=True
            )
    return norm_rows(final_rows, final_gain)


def solution(mesh):
    in_specs = (
        P("sp", None),
        P(),
        P(None, "sp", "tp"),
        P(None, "sp", "tp"),
        P(None, "sp", "tp"),
        P(None, "sp", "tp"),
        P(None, "tp"),
        P(),
    )
    out_specs = P(("sp", "tp"), None)
    return jax.shard_map(shards, mesh=mesh, in_specs=in_specs, out_specs=out_specs, check_vma=False)
```

profile of v0, /device:TPU:0, one launch (start us, length us, event | category | flops | bytes accessed | tf_op | source)
XLA Modules:
  0.0 580.5 jit_solution(9668719352871353835)
XLA Ops:
  10.4 3.3 fusion.9
  13.8 3.0 fusion.11
  17.3 2.3 fusion.19
  19.5 37.0 %all-gather.7.cloned.1.call-done = bf16[3,2048,128]{2,1,0:T(8,128)(2,1)} async-done(((bf16[3,256,128]{2,1,0:T(8,128)(2,1)}), bf16[3,2048,128]{2,1,0:T(8,128)(2,1)}) %all-gather.7.cloned.1.call-update) | async-done | bytes 1572880 | tf_op jit(solution)/shard_map/all_gather | solution.py:83
  56.5 3.8 convolution_multiply_fusion.5
  60.4 40.8 %all-gather.9.cloned.1.call-done = bf16[3,2048,128]{2,1,0:T(8,128)(2,1)} async-done(((bf16[3,256,128]{2,1,0:T(8,128)(2,1)}), bf16[3,2048,128]{2,1,0:T(8,128)(2,1)}) %all-gather.9.cloned.1.call-update) | async-done | bytes 1572880 | tf_op jit(solution)/shard_map/all_gather | solution.py:84
  101.3 3.8 convolution_convert_fusion.3
  105.1 1.3 collective-permute-start.1
  106.4 5.0 collective-permute-start
  111.6 2.7 collective-permute-done
  114.4 48.1 %all-gather.11.cloned.1.call-done = bf16[3,2048,256]{2,1,0:T(8,128)(2,1)} async-done(((bf16[3,256,256]{2,1,0:T(8,128)(2,1)}), bf16[3,2048,256]{2,1,0:T(8,128)(2,1)}) %all-gather.11.cloned.1.call-update) | async-done | bytes 3145744 | tf_op jit(solution)/shard_map/all_gather | solution.py:82
  162.4 3.8 convolution_multiply_fusion.2
  166.4 3.7 fusion.3
  170.2 4.7 fusion
  174.9 6.2 %fusion.24 = bf16[2,64,2,1024]{3,1,2,0:T(8,128)(2,1)S(1)} fusion(bf16[1280,2,64,1]{0,2,3,1:T(8,128)(2,1)S(1)} %bitcast.159, f32[2,1280,1024,2]{2,1,3,0:T(8,128)S(1)} %get-tuple-element.38, f32[2,2,1024]{2,1,0:T(2,128)S(1)} %exponential_add_fusion.2, f32[2,2,1024]{2,1,0:T(2,128)S(1)} %broadcast_maximum_fusion.2, pred[1024,1280]{0,1:T(8,128)(4,1)S(1)} %fusion.19), kind=kOutput, calls=%fused_computation.46 | convolution fusion | flops 697565184 | bytes 23166976 | tf_op jit(solution)/shard_map/kgqs,skd->qkgd/dot_general | solution.py:59
  181.1 42.1 %all-gather.13.cloned.1.call-done = bf16[3,2048,256]{2,1,0:T(8,128)(2,1)} async-done(((bf16[3,256,256]{2,1,0:T(8,128)(2,1)}), bf16[3,2048,256]{2,1,0:T(8,128)(2,1)}) %all-gather.13.cloned.1.call-update) | async-done | bytes 3145744 | tf_op jit(solution)/shard_map/all_gather | solution.py:85
  223.2 5.8 fusion.26
  229.1 70.2 %reduce-scatter.4.cloned.1.call-done = f32[256,2048]{1,0:T(8,128)} async-done(((f32[1024,2048]{1,0:T(8,128)}), f32[256,2048]{1,0:T(8,128)}) %reduce-scatter.4.cloned.1.call-update) | async-done | bytes 2097168 | tf_op jit(solution)/shard_map/reduce_scatter | solution.py:123
  299.2 2.7 convert_element_type.115
  302.3 34.3 %all-gather.15.cloned.1.call-done = bf16[1024,2048]{1,0:T(8,128)(2,1)} async-done(((bf16[256,2048]{1,0:T(8,128)(2,1)}), bf16[1024,2048]{1,0:T(8,128)(2,1)}) %all-gather.15.cloned.1.call-update) | async-done | bytes 4194320 | tf_op jit(solution)/shard_map/all_gather | solution.py:126
  336.6 3.2 fusion.12
  340.1 1.0 fusion.14
  341.1 2.7 convolution_multiply_fusion.4
  343.9 1.5 convolution_convert_fusion.2
  345.5 1.3 collective-permute-start.3
  346.8 4.5 collective-permute-start.2
  351.3 2.5 convolution_multiply_fusion.1
  354.9 3.7 fusion.4
  358.7 4.7 fusion.1
  363.4 7.8 %fusion.23 = bf16[2,64,2,1024]{3,1,2,0:T(8,128)(2,1)} fusion(bf16[1280,2,64,1]{0,2,3,1:T(8,128)(2,1)} %bitcast.161, f32[2,1280,1024,2]{2,1,3,0:T(8,128)S(1)} %get-tuple-element.40, f32[2,2,1024]{2,1,0:T(2,128)S(1)} %exponential_add_fusion.1, f32[2,2,1024]{2,1,0:T(2,128)S(1)} %broadcast_maximum_fusion.1, pred[1024,1280]{0,1:T(8,128)(4,1)S(1)} %fusion.19), kind=kOutput, calls=%fused_computation.45 | convolution fusion | flops 697565184 | bytes 23166976 | tf_op jit(solution)/shard_map/kgqs,skd->qkgd/dot_general | solution.py:59
  371.2 5.9 %fusion.25 = f32[1024,2048]{1,0:T(8,128)} fusion(bf16[1024,256]{0,1:T(8,128)(2,1)} %bitcast.158, bf16[3,2048,256]{2,1,0:T(8,128)(2,1)} %all-gather.13.cloned.1.call-done), kind=kOutput, calls=%fused_computation.56 | convolution fusion | flops 1073741824 | bytes 9961472 | tf_op jit(solution)/shard_map/dot_general | solution.py:118
  377.2 72.4 %reduce-scatter.6.cloned.1.call-done = f32[256,2048]{1,0:T(8,128)} async-done(((f32[1024,2048]{1,0:T(8,128)}), f32[256,2048]{1,0:T(8,128)}) %reduce-scatter.6.cloned.1.call-update) | async-done | bytes 2097168 | tf_op jit(solution)/shard_map/reduce_scatter | solution.py:123
  449.7 2.7 convert_element_type.123
  452.7 34.3 %all-gather.17.cloned.1.call-done = bf16[1024,2048]{1,0:T(8,128)(2,1)} async-done(((bf16[256,2048]{1,0:T(8,128)(2,1)}), bf16[1024,2048]{1,0:T(8,128)(2,1)}) %all-gather.17.cloned.1.call-update) | async-done | bytes 4194320 | tf_op jit(solution)/shard_map/all_gather | solution.py:126
  487.0 3.2 fusion.15
  490.5 1.0 fusion.17
  491.5 2.6 convolution_multiply_fusion.3
  494.2 1.5 convolution_convert_fusion.1
  495.7 1.3 collective-permute-start.5
  497.0 4.5 collective-permute-start.4
  501.6 2.5 convolution_multiply_fusion
  504.5 3.7 fusion.5
  508.2 4.7 fusion.2
  513.0 6.2 %fusion.22 = bf16[2,64,2,1024]{3,1,2,0:T(8,128)(2,1)S(1)} fusion(bf16[1280,2,64,1]{0,2,3,1:T(8,128)(2,1)S(1)} %bitcast.160, f32[2,1280,1024,2]{2,1,3,0:T(8,128)S(1)} %get-tuple-element.42, f32[2,2,1024]{2,1,0:T(2,128)S(1)} %exponential_add_fusion, f32[2,2,1024]{2,1,0:T(2,128)S(1)} %broadcast_maximum_fusion, pred[1024,1280]{0,1:T(8,128)(4,1)S(1)} %fusion.19), kind=kOutput, calls=%fused_computation.44 | convolution fusion | flops 697565184 | bytes 23166976 | tf_op jit(solution)/shard_map/kgqs,skd->qkgd/dot_general | solution.py:59
  519.2 4.5 convolution_convert_fusion
  523.7 45.7 %reduce-scatter.8.cloned.1.call-done = bf16[256,2048]{1,0:T(8,128)(2,1)} async-done(((bf16[1024,2048]{1,0:T(8,128)(2,1)}), bf16[256,2048]{1,0:T(8,128)(2,1)}) %reduce-scatter.8.cloned.1.call-update) | async-done | bytes 1048592 | tf_op jit(solution)/shard_map/reduce_scatter | solution.py:128
  569.4 1.5 fusion.20
  570.9 2.8 fusion.21
  (73 shorter events, 8.1 us)
Async XLA Ops:
  6.5 50.0 %all-gather.7.cloned.1.call-start = ((), (), s32[]{:S(2)}) async-start(), calls=%async_computation.3 | async-start | bytes 1769472 | tf_op jit(solution)/shard_map/all_gather | solution.py:83
  7.3 94.0 %all-gather.9.cloned.1.call-start = ((), (), s32[]{:S(2)}) async-start(), calls=%async_computation.4 | async-start | bytes 1769472 | tf_op jit(solution)/shard_map/all_gather | solution.py:84
  8.0 154.4 %all-gather.11.cloned.1.call-start = ((), (), s32[]{:S(2)}) async-start(), calls=%async_computation.5 | async-start | bytes 3538944 | tf_op jit(solution)/shard_map/all_gather | solution.py:82
  8.7 214.5 %all-gather.13.cloned.1.call-start = ((), (), s32[]{:S(2)}) async-start(), calls=%async_computation.6 | async-start | bytes 3538944 | tf_op jit(solution)/shard_map/all_gather | solution.py:85
  9.3 289.9 %reduce-scatter.4.cloned.1.call-start = ((), (), s32[]{:S(2)}) async-start(), calls=%async_computation.7 | async-start | bytes 10485760 | tf_op jit(solution)/shard_map/reduce_scatter | solution.py:123
  9.4 4.4 copy-start
  19.5 91.9 %copy-start.5 = (f32[3,4]{1,0:T(4,128)S(1)}, f32[3,4]{1,0:T(4,128)}, u32[]{:S(2)}) copy-start(f32[3,4]{1,0:T(4,128)} %param.14) | copy-start | bytes 148
  105.1 6.4 %collective-permute-start.1 = (bf16[128,256]{0,1:T(8,128)(2,1)S(1)}, bf16[128,256]{0,1:T(8,128)(2,1)S(1)}, u32[]{:S(2)}, u32[]{:S(2)}) collective-permute-start(bf16[128,256]{0,1:T(8,128)(2,1)S(1)} %get-tuple-element.31), channel_id=1, source_target_pairs={{4,0},{8,4},{12,8},{16,12},{20,16},{24,20},{28,24},{5,1},{9,5},{13... | collective-permute-start | bytes 196616 | tf_op jit(solution)/shard_map/ppermute | solution.py:21
  106.4 7.8 %collective-permute-start = (bf16[128,256]{0,1:T(8,128)(2,1)S(1)}, bf16[128,256]{0,1:T(8,128)(2,1)S(1)}, u32[]{:S(2)}, u32[]{:S(2)}) collective-permute-start(bf16[128,256]{0,1:T(8,128)(2,1)S(1)} %get-tuple-element.30), channel_id=1, source_target_pairs={{0,4},{4,8},{8,12},{12,16},{16,20},{20,24},{24,28},{1,5},{5,9},{9,... | collective-permute-start | bytes 196616 | tf_op jit(solution)/shard_map/ppermute | solution.py:18
  229.0 107.6 %all-gather.15.cloned.1.call-start = ((), (), s32[]{:S(2)}) async-start(), calls=%async_computation.8 | async-start | bytes 5242880 | tf_op jit(solution)/shard_map/all_gather | solution.py:126
  302.0 147.7 %reduce-scatter.6.cloned.1.call-start = ((), (), s32[]{:S(2)}) async-start(), calls=%async_computation.9 | async-start | bytes 10485760 | tf_op jit(solution)/shard_map/reduce_scatter | solution.py:123
  336.6 3.4 copy-start.2
  341.1 2.8 copy-start.3
  345.5 8.6 %collective-permute-start.3 = (bf16[128,256]{0,1:T(8,128)(2,1)S(1)}, bf16[128,256]{0,1:T(8,128)(2,1)S(1)}, u32[]{:S(2)}, u32[]{:S(2)}) collective-permute-start(bf16[128,256]{0,1:T(8,128)(2,1)S(1)} %get-tuple-element.29), channel_id=1, source_target_pairs={{4,0},{8,4},{12,8},{16,12},{20,16},{24,20},{28,24},{5,1},{9,5},{13... | collective-permute-start | bytes 196616 | tf_op jit(solution)/shard_map/ppermute | solution.py:21
  346.8 7.3 %collective-permute-start.2 = (bf16[128,256]{0,1:T(8,128)(2,1)S(1)}, bf16[128,256]{0,1:T(8,128)(2,1)S(1)}, u32[]{:S(2)}, u32[]{:S(2)}) collective-permute-start(bf16[128,256]{0,1:T(8,128)(2,1)S(1)} %get-tuple-element.28), channel_id=1, source_target_pairs={{0,4},{4,8},{8,12},{12,16},{16,20},{20,24},{24,28},{1,5},{5,9},{9,... | collective-permute-start | bytes 196616 | tf_op jit(solution)/shard_map/ppermute | solution.py:18
  377.2 109.8 %all-gather.17.cloned.1.call-start = ((), (), s32[]{:S(2)}) async-start(), calls=%async_computation.10 | async-start | bytes 5242880 | tf_op jit(solution)/shard_map/all_gather | solution.py:126
  452.4 117.0 %reduce-scatter.8.cloned.1.call-start = ((), (), s32[]{:S(2)}) async-start(), calls=%async_computation.11 | async-start | bytes 5242880 | tf_op jit(solution)/shard_map/reduce_scatter | solution.py:128
  487.0 3.4 copy-start.1
  495.7 8.6 %collective-permute-start.5 = (bf16[128,256]{0,1:T(8,128)(2,1)S(1)}, bf16[128,256]{0,1:T(8,128)(2,1)S(1)}, u32[]{:S(2)}, u32[]{:S(2)}) collective-permute-start(bf16[128,256]{0,1:T(8,128)(2,1)S(1)} %get-tuple-element.27), channel_id=1, source_target_pairs={{4,0},{8,4},{12,8},{16,12},{20,16},{24,20},{28,24},{5,1},{9,5},{13... | collective-permute-start | bytes 196616 | tf_op jit(solution)/shard_map/ppermute | solution.py:21
  497.0 7.3 %collective-permute-start.4 = (bf16[128,256]{0,1:T(8,128)(2,1)S(1)}, bf16[128,256]{0,1:T(8,128)(2,1)S(1)}, u32[]{:S(2)}, u32[]{:S(2)}) collective-permute-start(bf16[128,256]{0,1:T(8,128)(2,1)S(1)} %get-tuple-element.26), channel_id=1, source_target_pairs={{0,4},{4,8},{8,12},{12,16},{16,20},{20,24},{24,28},{1,5},{5,9},{9,... | collective-permute-start | bytes 196616 | tf_op jit(solution)/shard_map/ppermute | solution.py:18
  519.2 51.7 %copy-start.4 = (f32[2048]{0:T(1024)S(1)}, f32[2048]{0:T(1024)}, u32[]{:S(2)}) copy-start(f32[2048]{0:T(1024)} %param.15) | copy-start | bytes 24580
Sparse Core Ops, SparseCore 0:
  9.5 46.9 all-gather.6
  58.7 42.5 all-gather.8
  103.5 58.9 all-gather.10
  164.5 58.7 all-gather.12
  229.2 70.0 reduce-scatter.3
  302.1 34.4 all-gather.14
  377.3 72.3 reduce-scatter.5
  452.5 34.4 all-gather.16
  523.9 45.4 reduce-scatter.7
where the time goes:
time: 586 us; the launch traced here: 581 us
  waiting for transfers between devices  430 us (73%)
  matrix products  72.3 us (12%)
  other arithmetic  42.9 us (7%)
  starting transfers between devices  18.7 us (3%)
  between operations  13.9 us (2%)
    reduce_scatter x2, waiting for transfers between devices, shards(): lax.psum_scatter(project(), 'tp', scatter_dimension=0, tiled=True)  143 us
    all_gather x2, waiting for transfers between devices, shards(): current = lax.all_gather(share_rows, 'tp', axis=0, tiled=True)  68.6 us
    all_gather x1, waiting for transfers between devices, shards(): lax.all_gather(query_weight, 'sp', axis=1, tiled=True)  48.1 us
    reduce_scatter x1, waiting for transfers between devices, shards(): lax.psum_scatter(project().astype(jnp.bfloat16), 'tp', scatter_dimension=...  45.7 us
    all_gather x1, waiting for transfers between devices, shards(): lax.all_gather(output_weight, 'sp', axis=1, tiled=True)  42.1 us
    all_gather x1, waiting for transfers between devices, shards(): lax.all_gather(value_weight, 'sp', axis=1, tiled=True)  40.8 us
    all_gather x1, waiting for transfers between devices, shards(): lax.all_gather(key_weight, 'sp', axis=1, tiled=True)  37 us
    dot_general x3, matrix products, attend(): jnp.einsum('kgqs,skd->qkgd', weights, value_rows, preferred_element_type=...  20.2 us
  transfers between devices with their start and end apart: 15, of which 10 were waited for; matrix products, arithmetic and copies ran while one was open for 7% of the time, Pallas kernels for 0%

commit v1 on v0

--- a/solution.py
+++ b/solution.py
@@ -82,7 +82,7 @@
         lax.all_gather(query_weight, "sp", axis=1, tiled=True),
         lax.all_gather(key_weight, "sp", axis=1, tiled=True),
         lax.all_gather(value_weight, "sp", axis=1, tiled=True),
-        lax.all_gather(output_weight, "sp", axis=1, tiled=True),
+        jnp.concatenate(lax.all_gather(output_weight, "sp"), axis=1),
     )
     current = inputs
     final_rows = inputs

time: 586 us -> 598 us (1.020)
  transfers between devices with their start and end apart: 15 -> 15, of which waited for: 10 -> 10; matrix products, arithmetic and copies ran while one was open for 7% -> 6% of each run, Pallas kernels for 0% -> 0%
where the time goes in v1:
time: 598 us; the launch traced here: 593 us
  waiting for transfers between devices  434 us (73%)
  matrix products  74.8 us (13%)
  other arithmetic  43.5 us (7%)
  starting transfers between devices  18.7 us (3%)
  between operations  13.9 us (2%)
  local copies, waits for them, and re-layouts  8.21 us (1%)
    reduce_scatter x2, waiting for transfers between devices, shards(): lax.psum_scatter(project(), 'tp', scatter_dimension=0, tiled=True)  143 us
    all_gather x2, waiting for transfers between devices, shards(): current = lax.all_gather(share_rows, 'tp', axis=0, tiled=True)  68.6 us
    all_gather x1, waiting for transfers between devices, shards(): lax.all_gather(query_weight, 'sp', axis=1, tiled=True)  48.1 us
    all_gather x1, waiting for transfers between devices, shards(): lax.all_gather(output_weight, 'sp')  45.9 us
    reduce_scatter x1, waiting for transfers between devices, shards(): lax.psum_scatter(project().astype(jnp.bfloat16), 'tp', scatter_dimension=...  45.7 us
    all_gather x1, waiting for transfers between devices, shards(): lax.all_gather(value_weight, 'sp', axis=1, tiled=True)  40.8 us
    all_gather x1, waiting for transfers between devices, shards(): lax.all_gather(key_weight, 'sp', axis=1, tiled=True)  36.9 us
    dot_general x3, matrix products, attend(): jnp.einsum('kgqs,skd->qkgd', weights, value_rows, preferred_element_type=...  24.7 us
  transfers between devices with their start and end apart: 15, of which 10 were waited for; matrix products, arithmetic and copies ran while one was open for 6% of the time, Pallas kernels for 0%

profile of v1, /device:TPU:0, one launch (start us, length us, event | category | flops | bytes accessed | tf_op | source)
XLA Modules:
  0.0 593.0 jit_solution(16524265368742153774)
XLA Ops:
  10.4 3.3 fusion.9
  13.8 3.0 fusion.11
  17.3 2.3 fusion.19
  19.6 36.9 %all-gather.8.cloned.1.call-done = bf16[3,2048,128]{2,1,0:T(8,128)(2,1)} async-done(((bf16[3,256,128]{2,1,0:T(8,128)(2,1)}), bf16[3,2048,128]{2,1,0:T(8,128)(2,1)}) %all-gather.8.cloned.1.call-update) | async-done | bytes 1572880 | tf_op jit(solution)/shard_map/all_gather | solution.py:83
  56.5 3.8 convolution_multiply_fusion.5
  60.4 40.8 %all-gather.10.cloned.1.call-done = bf16[3,2048,128]{2,1,0:T(8,128)(2,1)} async-done(((bf16[3,256,128]{2,1,0:T(8,128)(2,1)}), bf16[3,2048,128]{2,1,0:T(8,128)(2,1)}) %all-gather.10.cloned.1.call-update) | async-done | bytes 1572880 | tf_op jit(solution)/shard_map/all_gather | solution.py:84
  101.3 3.8 convolution_convert_fusion.3
  105.1 1.3 collective-permute-start.1
  106.4 5.0 collective-permute-start
  111.6 2.7 collective-permute-done
  114.3 48.1 %all-gather.12.cloned.1.call-done = bf16[3,2048,256]{2,1,0:T(8,128)(2,1)} async-done(((bf16[3,256,256]{2,1,0:T(8,128)(2,1)}), bf16[3,2048,256]{2,1,0:T(8,128)(2,1)}) %all-gather.12.cloned.1.call-update) | async-done | bytes 3145744 | tf_op jit(solution)/shard_map/all_gather | solution.py:82
  162.4 3.8 convolution_multiply_fusion.2
  166.4 3.6 fusion.3
  170.1 4.6 fusion
  174.7 2.5 copy-done
  177.3 45.9 %all-gather.18.cloned.1.call-done = bf16[24,256,256]{2,1,0:T(8,128)(2,1)} async-done(((bf16[3,256,256]{2,1,0:T(8,128)(2,1)}), bf16[24,256,256]{2,1,0:T(8,128)(2,1)}) %all-gather.18.cloned.1.call-update) | async-done | bytes 3145744 | tf_op jit(solution)/shard_map/all_gather | solution.py:85
  223.2 3.1 fusion.49
  226.3 10.6 %fusion.24 = bf16[2,64,2,1024]{3,1,2,0:T(8,128)(2,1)S(1)} fusion(bf16[1280,2,64,1]{0,2,3,1:T(8,128)(2,1)S(1)} %bitcast.163, f32[2,1280,1024,2]{2,1,3,0:T(8,128)} %copy-done, f32[2,2,1024]{2,1,0:T(2,128)S(1)} %exponential_add_fusion.2, f32[2,2,1024]{2,1,0:T(2,128)S(1)} %broadcast_maximum_fusion.2, pred[1024,1280]{0,1:T(8,128)(4,1)S(1)} %fusion.19), kind=kOutput, calls=%fused_computation.46 | convolution fusion | flops 697565184 | bytes 23166976 | tf_op jit(solution)/shard_map/kgqs,skd->qkgd/dot_general | solution.py:59
  236.9 4.5 fusion.54
  241.5 70.2 %reduce-scatter.4.cloned.1.call-done = f32[256,2048]{1,0:T(8,128)} async-done(((f32[1024,2048]{1,0:T(8,128)}), f32[256,2048]{1,0:T(8,128)}) %reduce-scatter.4.cloned.1.call-update) | async-done | bytes 2097168 | tf_op jit(solution)/shard_map/reduce_scatter | solution.py:123
  311.7 2.8 convert_element_type.115
  314.7 34.3 %all-gather.14.cloned.1.call-done = bf16[1024,2048]{1,0:T(8,128)(2,1)} async-done(((bf16[256,2048]{1,0:T(8,128)(2,1)}), bf16[1024,2048]{1,0:T(8,128)(2,1)}) %all-gather.14.cloned.1.call-update) | async-done | bytes 4194320 | tf_op jit(solution)/shard_map/all_gather | solution.py:126
  349.1 3.2 fusion.12
  353.5 2.6 convolution_multiply_fusion.4
  356.2 2.6 convolution_convert_fusion.2
  358.8 1.3 collective-permute-start.3
  360.1 4.5 collective-permute-start.2
  364.7 2.5 convolution_multiply_fusion.1
  368.2 3.7 fusion.4
  372.0 4.7 fusion.1
  376.8 7.2 %fusion.23 = bf16[2,64,2,1024]{3,1,2,0:T(8,128)(2,1)S(1)} fusion(bf16[1280,2,64,1]{0,2,3,1:T(8,128)(2,1)} %bitcast.165, f32[2,1280,1024,2]{2,1,3,0:T(8,128)S(1)} %get-tuple-element.43, f32[2,2,1024]{2,1,0:T(2,128)S(1)} %exponential_add_fusion.1, f32[2,2,1024]{2,1,0:T(2,128)S(1)} %broadcast_maximum_fusion.1, pred[1024,1280]{0,1:T(8,128)(4,1)S(1)} %fusion.19), kind=kOutput, calls=%fused_computation.45 | convolution fusion | flops 697565184 | bytes 23166976 | tf_op jit(solution)/shard_map/kgqs,skd->qkgd/dot_general | solution.py:59
  383.9 4.5 fusion.55
  388.5 72.4 %reduce-scatter.6.cloned.1.call-done = f32[256,2048]{1,0:T(8,128)} async-done(((f32[1024,2048]{1,0:T(8,128)}), f32[256,2048]{1,0:T(8,128)}) %reduce-scatter.6.cloned.1.call-update) | async-done | bytes 2097168 | tf_op jit(solution)/shard_map/reduce_scatter | solution.py:123
  461.0 2.8 convert_element_type.123
  464.1 34.3 %all-gather.16.cloned.1.call-done = bf16[1024,2048]{1,0:T(8,128)(2,1)} async-done(((bf16[256,2048]{1,0:T(8,128)(2,1)}), bf16[1024,2048]{1,0:T(8,128)(2,1)}) %all-gather.16.cloned.1.call-update) | async-done | bytes 4194320 | tf_op jit(solution)/shard_map/all_gather | solution.py:126
  498.4 3.2 fusion.15
  502.9 2.6 convolution_multiply_fusion.3
  505.5 2.6 convolution_convert_fusion.1
  508.1 1.3 collective-permute-start.5
  509.4 4.5 collective-permute-start.4
  514.0 2.5 convolution_multiply_fusion
  516.8 3.7 fusion.5
  520.6 4.7 fusion.2
  526.0 6.9 %fusion.22 = bf16[2,64,2,1024]{3,1,2,0:T(8,128)(2,1)S(1)} fusion(bf16[1280,2,64,1]{0,2,3,1:T(8,128)(2,1)S(1)} %bitcast.164, f32[2,1280,1024,2]{2,1,3,0:T(8,128)S(1)} %get-tuple-element.45, f32[2,2,1024]{2,1,0:T(2,128)} %exponential_add_fusion, f32[2,2,1024]{2,1,0:T(2,128)} %copy-done.5, pred[1024,1280]{0,1:T(8,128)(4,1)S(1)} %fusion.19), kind=kOutput, calls=%fused_computation.44 | convolution fusion | flops 697565184 | bytes 23166976 | tf_op jit(solution)/shard_map/kgqs,skd->qkgd/dot_general | solution.py:59
  533.0 3.3 convolution_convert_fusion
  536.3 45.7 %reduce-scatter.8.cloned.1.call-done = bf16[256,2048]{1,0:T(8,128)(2,1)} async-done(((bf16[1024,2048]{1,0:T(8,128)(2,1)}), bf16[256,2048]{1,0:T(8,128)(2,1)}) %reduce-scatter.8.cloned.1.call-update) | async-done | bytes 1048592 | tf_op jit(solution)/shard_map/reduce_scatter | solution.py:128
  581.9 1.5 fusion.20
  583.5 2.8 fusion.21
  (78 shorter events, 10.7 us)
Async XLA Ops:
  6.5 50.0 %all-gather.8.cloned.1.call-start = ((), (), s32[]{:S(2)}) async-start(), calls=%async_computation.3 | async-start | bytes 1769472 | tf_op jit(solution)/shard_map/all_gather | solution.py:83
  7.3 94.0 %all-gather.10.cloned.1.call-start = ((), (), s32[]{:S(2)}) async-start(), calls=%async_computation.4 | async-start | bytes 1769472 | tf_op jit(solution)/shard_map/all_gather | solution.py:84
  8.0 154.4 %all-gather.12.cloned.1.call-start = ((), (), s32[]{:S(2)}) async-start(), calls=%async_computation.5 | async-start | bytes 3538944 | tf_op jit(solution)/shard_map/all_gather | solution.py:82
  8.7 214.4 %all-gather.18.cloned.1.call-start = ((), (), s32[]{:S(2)}) async-start(), calls=%async_computation.11 | async-start | bytes 3538944 | tf_op jit(solution)/shard_map/all_gather | solution.py:85
  9.3 302.3 %reduce-scatter.4.cloned.1.call-start = ((), (), s32[]{:S(2)}) async-start(), calls=%async_computation.6 | async-start | bytes 10485760 | tf_op jit(solution)/shard_map/reduce_scatter | solution.py:123
  9.4 4.4 copy-start.1
  19.5 91.9 %copy-start.7 = (f32[3,4]{1,0:T(4,128)S(1)}, f32[3,4]{1,0:T(4,128)}, u32[]{:S(2)}) copy-start(f32[3,4]{1,0:T(4,128)} %param.14) | copy-start | bytes 148
  105.1 6.4 %collective-permute-start.1 = (bf16[128,256]{0,1:T(8,128)(2,1)S(1)}, bf16[128,256]{0,1:T(8,128)(2,1)S(1)}, u32[]{:S(2)}, u32[]{:S(2)}) collective-permute-start(bf16[128,256]{0,1:T(8,128)(2,1)S(1)} %get-tuple-element.34), channel_id=1, source_target_pairs={{4,0},{8,4},{12,8},{16,12},{20,16},{24,20},{28,24},{5,1},{9,5},{13... | collective-permute-start | bytes 196616 | tf_op jit(solution)/shard_map/ppermute | solution.py:21
  106.4 7.8 %collective-permute-start = (bf16[128,256]{0,1:T(8,128)(2,1)S(1)}, bf16[128,256]{0,1:T(8,128)(2,1)S(1)}, u32[]{:S(2)}, u32[]{:S(2)}) collective-permute-start(bf16[128,256]{0,1:T(8,128)(2,1)S(1)} %get-tuple-element.33), channel_id=1, source_target_pairs={{0,4},{4,8},{8,12},{12,16},{16,20},{20,24},{24,28},{1,5},{5,9},{9,... | collective-permute-start | bytes 196616 | tf_op jit(solution)/shard_map/ppermute | solution.py:18
  170.0 7.2 %copy-start = (f32[2,1280,1024,2]{2,1,3,0:T(8,128)}, f32[2,1280,1024,2]{2,1,3,0:T(8,128)S(1)}, u32[]{:S(2)}) copy-start(f32[2,1280,1024,2]{2,1,3,0:T(8,128)S(1)} %get-tuple-element.41) | copy-start | bytes 62914564
  241.5 107.6 %all-gather.14.cloned.1.call-start = ((), (), s32[]{:S(2)}) async-start(), calls=%async_computation.7 | async-start | bytes 5242880 | tf_op jit(solution)/shard_map/all_gather | solution.py:126
  314.4 146.5 %reduce-scatter.6.cloned.1.call-start = ((), (), s32[]{:S(2)}) async-start(), calls=%async_computation.8 | async-start | bytes 10485760 | tf_op jit(solution)/shard_map/reduce_scatter | solution.py:123
  349.1 3.4 copy-start.3
  358.8 8.6 %collective-permute-start.3 = (bf16[128,256]{0,1:T(8,128)(2,1)S(1)}, bf16[128,256]{0,1:T(8,128)(2,1)S(1)}, u32[]{:S(2)}, u32[]{:S(2)}) collective-permute-start(bf16[128,256]{0,1:T(8,128)(2,1)S(1)} %get-tuple-element.32), channel_id=1, source_target_pairs={{4,0},{8,4},{12,8},{16,12},{20,16},{24,20},{28,24},{5,1},{9,5},{13... | collective-permute-start | bytes 196616 | tf_op jit(solution)/shard_map/ppermute | solution.py:21
  360.1 7.3 %collective-permute-start.2 = (bf16[128,256]{0,1:T(8,128)(2,1)S(1)}, bf16[128,256]{0,1:T(8,128)(2,1)S(1)}, u32[]{:S(2)}, u32[]{:S(2)}) collective-permute-start(bf16[128,256]{0,1:T(8,128)(2,1)S(1)} %get-tuple-element.31), channel_id=1, source_target_pairs={{0,4},{4,8},{8,12},{12,16},{16,20},{20,24},{24,28},{1,5},{5,9},{9,... | collective-permute-start | bytes 196616 | tf_op jit(solution)/shard_map/ppermute | solution.py:18
  388.5 109.9 %all-gather.16.cloned.1.call-start = ((), (), s32[]{:S(2)}) async-start(), calls=%async_computation.9 | async-start | bytes 5242880 | tf_op jit(solution)/shard_map/all_gather | solution.py:126
  463.7 118.2 %reduce-scatter.8.cloned.1.call-start = ((), (), s32[]{:S(2)}) async-start(), calls=%async_computation.10 | async-start | bytes 5242880 | tf_op jit(solution)/shard_map/reduce_scatter | solution.py:128
  498.4 3.4 copy-start.2
  508.1 8.6 %collective-permute-start.5 = (bf16[128,256]{0,1:T(8,128)(2,1)S(1)}, bf16[128,256]{0,1:T(8,128)(2,1)S(1)}, u32[]{:S(2)}, u32[]{:S(2)}) collective-permute-start(bf16[128,256]{0,1:T(8,128)(2,1)S(1)} %get-tuple-element.30), channel_id=1, source_target_pairs={{4,0},{8,4},{12,8},{16,12},{20,16},{24,20},{28,24},{5,1},{9,5},{13... | collective-permute-start | bytes 196616 | tf_op jit(solution)/shard_map/ppermute | solution.py:21
  509.4 7.3 %collective-permute-start.4 = (bf16[128,256]{0,1:T(8,128)(2,1)S(1)}, bf16[128,256]{0,1:T(8,128)(2,1)S(1)}, u32[]{:S(2)}, u32[]{:S(2)}) collective-permute-start(bf16[128,256]{0,1:T(8,128)(2,1)S(1)} %get-tuple-element.29), channel_id=1, source_target_pairs={{0,4},{4,8},{8,12},{12,16},{16,20},{20,24},{24,28},{1,5},{5,9},{9,... | collective-permute-start | bytes 196616 | tf_op jit(solution)/shard_map/ppermute | solution.py:18
  520.6 4.7 copy-start.5
  526.0 7.0 %copy-start.4 = (bf16[1,8,256,256]{3,2,0,1:T(8,128)(2,1)S(1)}, bf16[1,8,256,256]{3,2,0,1:T(8,128)(2,1)}, u32[]{:S(2)}) copy-start(bf16[1,8,256,256]{3,2,0,1:T(8,128)(2,1)} %get-tuple-element.8) | copy-start | bytes 3145732
  533.0 50.5 %copy-start.6 = (f32[2048]{0:T(1024)S(1)}, f32[2048]{0:T(1024)}, u32[]{:S(2)}) copy-start(f32[2048]{0:T(1024)} %param.15) | copy-start | bytes 24580
Sparse Core Ops, SparseCore 0:
  9.5 46.9 all-gather.7
  58.7 42.5 all-gather.9
  103.5 58.9 all-gather.11
  164.5 58.6 all-gather.17
  241.6 70.0 reduce-scatter.3
  314.6 34.4 all-gather.13
  388.6 72.3 reduce-scatter.5
  463.9 34.4 all-gather.15
  536.4 45.5 reduce-scatter.7
